TPU v7x, 128 devices: a whole 4x4x4 slice. The times are simulated.
128 devices in a mesh: sp: 64 (over z, y, x), tp: 2 (over core).
Axes of the slice: x: 4, y: 4, z: 4, core: 2. Of those that a mesh axis runs over, the one named last changes fastest.
Arguments:
- mixer_value_rows: bfloat16 [16384, 2048], P('sp', 'tp'), may hold values from -6 to 6
- input_map_rows: bfloat16 [16384, 256], P('sp', 'tp'), may hold values from -6 to 6
- output_map_rows: bfloat16 [16384, 256], P('sp', 'tp'), may hold values from -6 to 6
- gate_preactivation: bfloat16 [16384, 2048], P('sp', 'tp'), may hold values from -25 to 25
- step_preactivation: float32 [16384, 32], P('sp', 'tp'), may hold values from -4 to 4
- position_extra_decay: float32 [16384, 32], P('sp', 'tp'), may hold values from -0.69 to 0
- head_decay_rate: float32 [32], P('tp'), may hold values from 7.8125e-05 to 0.08
- head_direct_term: float32 [32], P('tp'), may hold values from -2.5 to 2.5
- value_taps: bfloat16 [4, 2048], P(None, 'tp'), may hold values from -3 to 3
- input_map_taps: bfloat16 [4, 256], P(None, 'tp'), may hold values from -3 to 3
- output_map_taps: bfloat16 [4, 256], P(None, 'tp'), may hold values from -3 to 3
- document_index: int32 [16384], P('sp'), may hold values from 0 to 15, never falling along the last dimension, each value on 1 to 1536 neighbouring positions
- gated_norm_gain: float32 [2048], replicated, may hold values from 0.1 to 1.9
- residual: bfloat16 [16384, 2048], P(('sp', 'tp')), may hold values from -6 to 6
- mixer_output_weight: bfloat16 [2048, 2048], replicated, may hold values from -0.125 to 0.125
- expert_norm_gain: float32 [2048], replicated, may hold values from 0.1 to 1.9
- expert_group_weight: float32 [16384, 4], P(('sp', 'tp')), may hold values from 0.5 to 2
- chosen_expert_weight: float32 [16384, 2], P(('sp', 'tp')), may hold values from 0.5 to 2
- chosen_expert_index: int32 [16384, 2], P(('sp', 'tp')), may hold values from 0 to 127, all different within a row; in each aligned block of 128 rows (0 to 127, 128 to 255, ...) at most 4 rows name the same one
- expert_gate_weight: bfloat16 [128, 2048, 512], P(('sp', 'tp')), may hold values from -0.125 to 0.125
- expert_up_weight: bfloat16 [128, 2048, 512], P(('sp', 'tp')), may hold values from -0.125 to 0.125
- expert_down_weight: bfloat16 [128, 512, 2048], P(('sp', 'tp')), may hold values from -0.25 to 0.25
Outputs:
- output: bfloat16 [16384, 2048], P(('sp', 'tp'))
Inputs may be any that keep to these rules, and one draw needn't show every extreme that they name: `document_index`: document numbers never fall along the sequence; a document holds 1 to 1536 positions. `chosen_expert_index`: the 2 entries of a row differ. Among the rows of one device (aligned blocks of 128 rows) no expert is named by more than 4 rows, a bound that some expert reaches in some blocks.
All inputs are finite; a program needn't handle non-finite values.
Results may differ from a plain program's by a relative error of at most 0.019.
Values may be sent and summed in bfloat16 or wider, within the bound.
No kernel may reach another device: no remote copies, remote signals or barrier semaphores. Data moves between devices by JAX's collectives and lax.ppermute only.
A program may use at most 128 MiB of HBM per device.

v0:
```python
import jax
import jax.numpy as jnp
from jax import lax
from jax.sharding import Mesh
from jax.sharding import PartitionSpec as P

D_SSM = 2048
HEAD_DIM = 64
D_STATE = 128
BLOCK = 128
EXPERT_GROUPS = 4
SP = ("sp_0", "sp_1", "sp_2")
SP_TP = ("sp_0", "sp_1", "sp_2", "tp")


EPSILON = 1e-06


def shifted(block, axis, distance):
    devices = range(lax.axis_size(axis))
    route = [(i - distance, i) for i in devices if i - distance in devices]
    return lax.ppermute(block, axis, route)


def neutral_like(array, identity):
    return jax.tree.map(
        lambda a, e: jnp.broadcast_to(jnp.asarray(e, a.dtype), a.shape), array, identity
    )


def carried_in_2(array, axes, combine, identity):
    before = start = neutral_like(array, identity)
    subtotal = array
    for axis in reversed(axes):
        count, position = (lax.axis_size(axis), lax.axis_index(axis))
        pieces = jax.tree.map(
            lambda part, kind: lax.all_gather(part.astype(kind), axis),
            subtotal,
            (jnp.bfloat16, jnp.bfloat16, jnp.bfloat16),
        )
        inside, subtotal = (start, start)
        for k in range(count):
            passed = k < position
            subtotal = combine(
                subtotal, jax.tree.map(lambda part, own: part[k].astype(own.dtype), pieces, array)
            )
            inside = jax.tree.map(lambda new, old: jnp.where(passed, new, old), subtotal, inside)
        before = combine(inside, before)
    return before


def copy_for_each(array, axis):
    count = lax.axis_size(axis)
    return lax.all_to_all(
        jnp.broadcast_to(array[None], (count, *array.shape)), axis, 0, 0, tiled=True
    )


def taken_together(array, axis):
    everything = copy_for_each(array, axis)
    return jnp.sum(everything, axis=0)


def cut_along(array, dim, count):
    before, after = (array.shape[:dim], array.shape[dim + 1 :])
    return jnp.moveaxis(array.reshape(*before, count, -1, *after), dim, 0)


def sum_at_owner(array, axis, dim):
    count = lax.axis_size(axis)
    tiles = lax.all_to_all(cut_along(array, dim, count), axis, 0, 0, tiled=True)
    return jnp.sum(tiles.astype(jnp.float32), axis=0)


def joined_along(tiles, dim):
    tiles = jnp.moveaxis(tiles, 0, dim)
    lengths = tiles.shape
    return tiles.reshape(*lengths[:dim], lengths[dim] * lengths[dim + 1], *lengths[dim + 2 :])


def joined_exchange(array, axis, axes, splits, concats):
    sizes = [lax.axis_size(a) for a in axes]
    tiles = cut_along(array, splits[0], sizes[0])
    tiles = jnp.moveaxis(cut_along(tiles, splits[1] + 1, sizes[1]), 0, 1)
    inside = tiles.shape[2:]
    tiles = tiles.reshape(-1, *inside)
    tiles = lax.all_to_all(tiles, axis, split_axis=0, concat_axis=0, tiled=True)
    tiles = joined_along(tiles.reshape(*sizes, *inside), concats[0] + 1)
    return joined_along(tiles, concats[1])


def conv_silu(previous, source_rows, weights, prev_docs, documents):
    kernel = weights.shape[0]
    length = source_rows.shape[0]
    padded = jnp.concatenate([previous, source_rows], axis=0).astype(jnp.float32)
    pad_docs = jnp.concatenate([prev_docs, documents])
    summed = jnp.zeros(source_rows.shape, jnp.float32)
    for offset in range(kernel):
        same_doc = (pad_docs[offset : offset + length] == documents).astype(jnp.float32)
        summed = (
            summed
            + weights[offset].astype(jnp.float32)[None, :]
            * padded[offset : offset + length]
            * same_doc[:, None]
        )
    return jax.nn.silu(summed).astype(jnp.bfloat16)


def scaled_norm(values, gain_vector):
    widened = values.astype(jnp.float32)
    factor = lax.rsqrt(jnp.mean(widened * widened, axis=-1, keepdims=True) + EPSILON)
    return (widened * factor * gain_vector[None, :]).astype(jnp.bfloat16)


def block_step(carried_pair, pieces):
    carried, last_doc = carried_pair
    step_values, decay_block, b_block, c_block, doc_block = pieces
    length = step_values.shape[0]
    cumulative = jnp.cumsum(decay_block, axis=0)
    causal = jnp.arange(length)[:, None] >= jnp.arange(length)[None, :]
    allowed = causal & (doc_block[:, None] == doc_block[None, :])
    cum_heads = jnp.transpose(cumulative, (1, 2, 0))
    spread = cum_heads[:, :, :, None] - cum_heads[:, :, None, :]
    kernel_mat = jnp.exp(jnp.where(allowed[None, None], spread, -jnp.inf))
    scores = jnp.einsum("lgn,sgn->gls", c_block, b_block, preferred_element_type=jnp.float32)
    weighted = (scores[:, None] * kernel_mat).astype(jnp.bfloat16)
    inside = jnp.einsum(
        "grls,sgrp->lgrp", weighted, step_values, preferred_element_type=jnp.float32
    )
    entering = (doc_block == last_doc).astype(jnp.float32)
    readout = jnp.einsum(
        "lgn,grpn->lgrp", c_block, carried.astype(jnp.bfloat16), preferred_element_type=jnp.float32
    )
    inside = inside + readout * (jnp.exp(cumulative) * entering[:, None, None])[..., None]
    tail_mask = (doc_block == doc_block[-1]).astype(jnp.float32)
    end_decay = jnp.exp(cumulative[-1][None] - cumulative) * tail_mask[:, None, None]
    end_values = (end_decay[..., None] * step_values.astype(jnp.float32)).astype(jnp.bfloat16)
    fresh_state = jnp.einsum(
        "lgn,lgrp->grpn", b_block, end_values, preferred_element_type=jnp.float32
    )
    keep_flag = (doc_block[-1] == last_doc).astype(jnp.float32)
    fresh_state = fresh_state + carried * (jnp.exp(cumulative[-1]) * keep_flag)[..., None, None]
    return ((fresh_state, doc_block[-1]), inside)


def join_states(earlier, latter):
    early_state, early_log, early_reset = earlier
    late_state, late_log, late_reset = latter
    passing = 1.0 - late_reset
    factor = jnp.exp(late_log) * passing
    return (
        late_state + factor[:, :, None, None] * early_state,
        late_log + passing * early_log,
        jnp.maximum(early_reset, late_reset),
    )


def local(
    mixer_value_rows,
    input_map_rows,
    output_map_rows,
    gate_preactivation,
    step_preactivation,
    position_extra_decay,
    head_decay_rate,
    head_direct_term,
    value_taps,
    input_map_taps,
    output_map_taps,
    document_index,
    gated_norm_gain,
    residual,
    mixer_output_weight,
    expert_norm_gain,
    expert_group_weight,
    chosen_expert_weight,
    chosen_expert_index,
    expert_gate_weight,
    expert_up_weight,
    expert_down_weight,
):
    kernel = value_taps.shape[0]
    documents = document_index + 1
    edge_rows = (
        mixer_value_rows[-(kernel - 1) :],
        input_map_rows[-(kernel - 1) :],
        output_map_rows[-(kernel - 1) :],
        documents[-(kernel - 1) :].astype(jnp.bfloat16),
    )
    prev_value, prev_input, prev_output, prev_marks = shifted(
        (edge_rows[0], edge_rows[1], edge_rows[2], edge_rows[3]), SP, 1
    )
    prev_docs = prev_marks.astype(jnp.int32)
    value_conv = conv_silu(prev_value, mixer_value_rows, value_taps, prev_docs, documents)
    input_conv = conv_silu(prev_input, input_map_rows, input_map_taps, prev_docs, documents)
    output_conv = conv_silu(prev_output, output_map_rows, output_map_taps, prev_docs, documents)
    length = mixer_value_rows.shape[0]
    groups = input_map_rows.shape[1] // D_STATE
    head_count = step_preactivation.shape[1]
    per_group = head_count // groups
    blocks = length // BLOCK
    head_step_length = jax.nn.softplus(step_preactivation)
    decay_logarithm = position_extra_decay - head_step_length * head_decay_rate[None, :]
    value_heads = value_conv.astype(jnp.float32).reshape(length, groups, per_group, HEAD_DIM)
    step_values = (
        value_heads * head_step_length.reshape(length, groups, per_group)[..., None]
    ).astype(jnp.bfloat16)
    last_prev = prev_docs[-1]
    initial = (jnp.zeros((groups, per_group, HEAD_DIM, D_STATE), jnp.float32), last_prev)
    ended, outputs = lax.scan(
        block_step,
        initial,
        (
            step_values.reshape(blocks, BLOCK, groups, per_group, HEAD_DIM),
            decay_logarithm.reshape(blocks, BLOCK, groups, per_group),
            input_conv.reshape(blocks, BLOCK, groups, D_STATE),
            output_conv.reshape(blocks, BLOCK, groups, D_STATE),
            documents.reshape(blocks, BLOCK),
        ),
    )
    local_state = ended[0]
    cumulative = jnp.cumsum(decay_logarithm, axis=0)
    tail_mask = (documents == documents[-1]).astype(jnp.float32)
    tail_log = jnp.sum(decay_logarithm * tail_mask[:, None], axis=0).reshape(groups, per_group)
    reset_flag = (documents[-1] != last_prev).astype(jnp.float32)
    identity = (jnp.zeros_like(local_state), jnp.zeros_like(tail_log), jnp.zeros((), jnp.float32))
    incoming = carried_in_2((local_state, tail_log, reset_flag), SP, join_states, identity)[0]
    entering = (documents == last_prev).astype(jnp.float32)
    c_groups = output_conv.reshape(length, groups, D_STATE)
    readout = jnp.einsum(
        "lgn,grpn->lgrp",
        c_groups,
        incoming.astype(jnp.bfloat16),
        preferred_element_type=jnp.float32,
    )
    carried_in = (
        readout
        * (jnp.exp(cumulative).reshape(length, groups, per_group) * entering[:, None, None])[
            ..., None
        ]
    )
    mixer_out = outputs.reshape(length, groups, per_group, HEAD_DIM) + carried_in
    mixer_out = (
        mixer_out + value_heads * head_direct_term.reshape(groups, per_group)[None, :, :, None]
    )
    gated_rows = (
        mixer_out.reshape(length, head_count * HEAD_DIM)
        * jax.nn.silu(gate_preactivation.astype(jnp.float32))
    ).astype(jnp.bfloat16)
    widened = gated_rows.astype(jnp.float32)
    squares = taken_together(jnp.sum(widened * widened, axis=1), "tp")
    factor = lax.rsqrt(squares / D_SSM + EPSILON)
    local_width = gated_rows.shape[1]
    first_col = lax.axis_index("tp") * local_width
    local_gain = lax.dynamic_slice_in_dim(gated_norm_gain, first_col, local_width, 0)
    normed = (widened * factor[:, None] * local_gain[None, :]).astype(jnp.bfloat16)
    local_rows = lax.dynamic_slice_in_dim(mixer_output_weight, first_col, local_width, 0)
    projected = sum_at_owner(
        jnp.dot(normed, local_rows, preferred_element_type=jnp.float32).astype(jnp.bfloat16),
        "tp",
        0,
    )
    mixed_rows = (residual.astype(jnp.float32) + projected).astype(jnp.bfloat16)
    ffn_in = scaled_norm(mixed_rows, expert_norm_gain)
    experts = lax.axis_size(SP) * lax.axis_size("tp")
    row_count = ffn_in.shape[0]
    width = ffn_in.shape[1]
    choose = chosen_expert_index.shape[1]
    capacity = 2 * length // experts
    flat_ids = chosen_expert_index.reshape(-1)
    onehot = (flat_ids[:, None] == jnp.arange(experts, dtype=jnp.int32)[None, :]).astype(jnp.int32)
    ranking = jnp.sum((jnp.cumsum(onehot, axis=0) - onehot) * onehot, axis=1)
    slot_index = flat_ids * capacity + ranking
    owners = jnp.arange(row_count * choose, dtype=jnp.int32) // choose
    outgoing = (
        jnp.zeros((experts * capacity, width), jnp.bfloat16).at[slot_index].set(ffn_in[owners])
    )
    sectioned = outgoing.reshape(lax.axis_size(SP), lax.axis_size("tp"), capacity, width)
    arrived = joined_exchange(sectioned, SP_TP, (SP, "tp"), (0, 1), (0, 1))
    arrived_shape = arrived.shape
    flat_rows = arrived.reshape(-1, width)
    gate_part = jnp.dot(flat_rows, expert_gate_weight[0], preferred_element_type=jnp.float32)
    upward = jnp.dot(flat_rows, expert_up_weight[0], preferred_element_type=jnp.float32)
    hidden = (jax.nn.silu(gate_part) * upward).astype(jnp.bfloat16)
    finished = (
        jnp.dot(hidden, expert_down_weight[0], preferred_element_type=jnp.float32)
        .astype(jnp.bfloat16)
        .reshape(arrived_shape)
    )
    returned = joined_exchange(finished, SP_TP, (SP, "tp"), (0, 1), (0, 1))
    answers = returned.reshape(experts * capacity, width)[slot_index].reshape(
        row_count, choose, width
    )
    per_expert_group = experts // EXPERT_GROUPS
    owner_group = chosen_expert_index // per_expert_group
    group_pick = (
        owner_group[:, :, None] == jnp.arange(EXPERT_GROUPS, dtype=jnp.int32)[None, None, :]
    ).astype(jnp.float32)
    route_weight = (
        jnp.sum(group_pick * expert_group_weight[:, None, :], axis=2) * chosen_expert_weight
    )
    summed = mixed_rows.astype(jnp.float32) + jnp.sum(
        route_weight[:, :, None] * answers.astype(jnp.float32), axis=1
    )
    return summed.astype(jnp.bfloat16)


def solution(mesh):
    torus = Mesh(mesh.devices.reshape(4, 4, 4, mesh.shape["tp"]), ("sp_0", "sp_1", "sp_2", "tp"))
    in_specs = (
        P(SP, "tp"),
        P(SP, "tp"),
        P(SP, "tp"),
        P(SP, "tp"),
        P(SP, "tp"),
        P(SP, "tp"),
        P("tp"),
        P("tp"),
        P(None, "tp"),
        P(None, "tp"),
        P(None, "tp"),
        P(SP),
        P(),
        P(SP_TP, None),
        P(),
        P(),
        P(SP_TP, None),
        P(SP_TP, None),
        P(SP_TP, None),
        P(SP_TP, None, None),
        P(SP_TP, None, None),
        P(SP_TP, None, None),
    )
    out_specs = P(SP_TP, None)
    return jax.shard_map(local, mesh=torus, in_specs=in_specs, out_specs=out_specs, check_vma=False)
```

profile of v0, /device:TPU:1, one launch (start us, length us, event | category | flops | bytes accessed | tf_op | source)
XLA Modules:
  0.0 315.6 jit_solution(4690262849737791489)
XLA Ops:
  7.5 3.9 %collective-permute-start = (bf16[3]{0:T(256)(128)(2,1)S(1)}, bf16[3]{0:T(256)(128)(2,1)S(1)}, u32[]{:S(2)}, u32[]{:S(2)}) collective-permute-start(bf16[3]{0:T(256)(128)(2,1)S(1)} %slice.237), channel_id=1, source_target_pairs={{0,2},{2,4},{4,6},{6,8},{8,10},{10,12},{12,14},{14,16},{16,18},{18... | collective-permute-start | bytes 26 | tf_op jit(solution)/shard_map/ppermute | solution.py:22
  12.1 3.1 collective-permute-start.1
  15.9 2.8 collective-permute-start.3
  19.4 3.1 collective-permute-start.2
  25.6 2.0 compare_convert_fusion.8
  27.5 0.9 multiply_reduce_fusion.1
  31.4 1.8 fusion.96
  33.2 2.5 copy.120
  35.8 2.8 reshape.912
  38.5 1.7 multiply_convert_fusion.3
  41.2 39.4 %while.15 = (s32[]{:T(128)}, f32[1,16,64,128]{3,2,1,0:T(8,128)S(1)}, s32[]{:T(128)}, f32[2,128,1,16,64]{1,0,4,3,2:T(2,128)}, f32[2,128,1,16]{3,1,2,0:T(8,128)S(1...) while((s32[]{:T(128)}, ...), condition=%wide.region_2.3_spmd.clone, body=%wide.region_0.2_spmd.clone.sunk | while | flops 107401744 | bytes 5144061 | solution.py:210
  43.4 1.2 fusion.204
  44.9 2.3 fusion.208
  47.2 13.1 %dynamic_update_slice.6 = f32[2,128,1,16,64]{1,0,4,3,2:T(2,128)} dynamic-update-slice(f32[2,128,1,16,64]{1,0,4,3,2:T(2,128)} %get-tuple-element.299, f32[1,128,1,16,64]{1,0,4,3,2:T(1,128)} %bitcast.336, s32[]{:T(128)S(6)} %copy.165, s32[]{:T(128)} %constant.106.clone.1..sunk, s32[]{:T(128)} %constant.106.clone.1..sunk, s32[]{:T(128)} %constant.106.clone.1..sunk, s32[]{:T(128)} %constant.106.clone.1..sunk) | dynamic-update-slice | bytes 1048580 | tf_op jit(solution)/shard_map/while/body/jit(dynamic_update_index_in_dim)/dynamic_update_slice | solution.py:210
  63.1 1.2 fusion.204
  64.6 2.3 fusion.208
  66.9 13.1 %dynamic_update_slice.6 = f32[2,128,1,16,64]{1,0,4,3,2:T(2,128)} dynamic-update-slice(f32[2,128,1,16,64]{1,0,4,3,2:T(2,128)} %get-tuple-element.299, f32[1,128,1,16,64]{1,0,4,3,2:T(1,128)} %bitcast.336, s32[]{:T(128)S(6)} %copy.165, s32[]{:T(128)} %constant.106.clone.1..sunk, s32[]{:T(128)} %constant.106.clone.1..sunk, s32[]{:T(128)} %constant.106.clone.1..sunk, s32[]{:T(128)} %constant.106.clone.1..sunk) | dynamic-update-slice | bytes 1048580 | tf_op jit(solution)/shard_map/while/body/jit(dynamic_update_index_in_dim)/dynamic_update_slice | solution.py:210
  84.7 8.5 %all-reduce.4 = (bf16[4]{0:T(256)(128)(2,1)S(1)}, bf16[64]{0:T(256)(128)(2,1)S(1)}) all-reduce(bf16[4]{0:T(256)(128)(2,1)S(1)} %dynamic-update-slice.1, bf16[64]{0:T(256)(128)(2,1)S(1)} %dynamic-update-slice), channel_id=1, replica_groups=mesh['sp_0'=4,'sp_1'=4,'sp_2'=4,'tp'=2] {'sp_2'}, use_global_device_ids=true, to_apply=%add.1 | all-reduce | flops 68 | bytes 272
  98.7 8.0 %all-gather.10.cloned.1.call-done = bf16[4,16,64,128]{3,2,1,0:T(8,128)(2,1)} async-done(((bf16[1,16,64,128]{3,2,1,0:T(8,128)(2,1)}), bf16[4,16,64,128]{3,2,1,0:T(8,128)(2,1)}) %all-gather.10.cloned.1.call-update) | async-done | bytes 1048592 | tf_op jit(solution)/shard_map/all_gather | solution.py:37
  106.7 2.3 fusion.95
  111.1 8.4 %all-reduce.2 = bf16[4]{0:T(256)(128)(2,1)S(1)} all-reduce(bf16[4]{0:T(256)(128)(2,1)S(1)} %dynamic-update-slice.2), channel_id=1, replica_groups=mesh['sp_0'=4,'sp_1'=4,'sp_2'=4,'tp'=2] {'sp_1'}, use_global_device_ids=true, to_apply=%add.2 | all-reduce | flops 4 | bytes 16
  119.5 5.2 %all_gather.50 = bf16[4,1,16]{2,1,0:T(2,128)(2,1)S(1)} all-gather(bf16[1,1,16]{2,1,0:T(2,128)(2,1)S(1)} %get-tuple-element.201), channel_id=1, replica_groups=mesh['sp_0'=4,'sp_1'=4,'sp_2'=4,'tp'=2] {'sp_1'}, dimensions={0}, use_global_device_ids=true | all-gather | bytes 160 | tf_op jit(solution)/shard_map/all_gather | solution.py:37
  130.3 3.3 %all-gather.6.cloned.1.call-done = bf16[4,1,16,64,128]{4,3,2,1,0:T(8,128)(2,1)} async-done(((bf16[1,1,16,64,128]{4,3,2,1,0:T(8,128)(2,1)}), bf16[4,1,16,64,128]{4,3,2,1,0:T(8,128)(2,1)}) %all-gather.6.cloned.1.call-update) | async-done | bytes 1048592 | tf_op jit(solution)/shard_map/all_gather | solution.py:37
  133.6 2.3 fusion.94
  138.0 8.6 %all-reduce.3 = bf16[4]{0:T(256)(128)(2,1)S(1)} all-reduce(bf16[4]{0:T(256)(128)(2,1)S(1)} %dynamic-update-slice.3), channel_id=1, replica_groups=mesh['sp_0'=4,'sp_1'=4,'sp_2'=4,'tp'=2] {'sp_0'}, use_global_device_ids=true, to_apply=%add.3 | all-reduce | flops 4 | bytes 16
  146.6 5.2 %all_gather.54 = bf16[4,1,16]{2,1,0:T(2,128)(2,1)S(1)} all-gather(bf16[1,1,16]{2,1,0:T(2,128)(2,1)S(1)} %get-tuple-element.159), channel_id=1, replica_groups=mesh['sp_0'=4,'sp_1'=4,'sp_2'=4,'tp'=2] {'sp_0'}, dimensions={0}, use_global_device_ids=true | all-gather | bytes 160 | tf_op jit(solution)/shard_map/all_gather | solution.py:37
  155.9 3.1 reshape.915
  159.0 1.7 all-gather.8.cloned.1.call-done
  160.7 4.7 %fusion.52 = f32[256,1,16,64]{0,3,2,1:T(8,128)} fusion(f32[256,1,16,64]{0,3,2,1:T(8,128)} %reshape.915, f32[256,1,16,64]{0,3,2,1:T(8,128)} %bitcast.340, f32[16]{0:T(128)S(1)} %copy-done.8, f32[256,16]{0,1:T(8,128)S(1)} %fusion.147, bf16[4,1,16,64,128]{4,3,2,1,0:T(8,128)(2,1)} %all-gather.8.cloned.1.call-done, f32[16]{0:T(128)S(1)} %get-tuple-element.203, ...), kind=kOutput, calls=%fused_computation.71 | convolution fusion | flops 74711040 | bytes 6374348 | tf_op jit(solution)/shard_map/lgn,grpn->lgrp/dot_general | solution.py:230
  165.4 2.6 copy.126
  168.0 1.6 fusion.60
  169.7 8.6 %all_to_all.21 = f32[2,1,256]{2,1,0:T(1,128)S(1)} all-to-all(f32[2,1,256]{2,1,0:T(1,128)S(1)} %broadcast_in_dim.18), channel_id=1, replica_groups=mesh['sp_0'=4,'sp_1'=4,'sp_2'=4,'tp'=2] {'tp'}, dimensions={0} | all-to-all | bytes 4096 | tf_op jit(solution)/shard_map/all_to_all | solution.py:54
  178.4 3.5 %fusion.39 = bf16[256,2048]{1,0:T(8,128)(2,1)S(1)} fusion(bf16[2048,2048]{1,0:T(8,128)(2,1)} %param.38, s32[]{:T(128)} %select_n.371, bf16[256,1024]{1,0:T(8,128)(2,1)S(1)} %get-tuple-element.155, f32[1024]{0:T(1024)S(1)} %dynamic-slice-done, f32[256]{0:T(256)S(1)} %add_rsqrt_fusion), kind=kOutput, calls=%fused_computation.56 | convolution fusion | flops 1075314688 | bytes 5772800 | tf_op jit(solution)/shard_map/dot_general | solution.py:259
  181.9 4.7 %all_to_all.22 = bf16[2,128,2048]{2,1,0:T(8,128)(2,1)S(1)} all-to-all(bf16[2,128,2048]{2,1,0:T(8,128)(2,1)S(1)} %bitcast.346), channel_id=1, replica_groups=mesh['sp_0'=4,'sp_1'=4,'sp_2'=4,'tp'=2] {'tp'}, dimensions={0} | all-to-all | bytes 2097152 | tf_op jit(solution)/shard_map/all_to_all | solution.py:71
  187.5 7.0 %scatter_custom_fusion = bf16[512,2048]{1,0:T(8,128)(2,1)} fusion(s32[256]{0:T(256)S(1)} %bitcast.356, bf16[128,2048]{1,0:T(8,128)(2,1)S(1)} %fusion.65, s32[1024]{0:T(1024)S(1)} %pad_clamp_fusion.1, bf16[]{:T(256)} %constant.124.clone.1), kind=kCustom, calls=%fused_computation.98 | custom fusion | bytes 2097154 | tf_op jit(solution)/shard_map/scatter | solution.py:276
  194.5 4.1 %reshape_transpose_transpose_reshape_reshape_reshape.6 = bf16[128,1,1,4,2048]{4,3,2,1,0:T(4,128)(2,1)} reshape(bf16[512,2048]{1,0:T(8,128)(2,1)} %scatter_custom_fusion) | data formatting | bytes 4194304 | tf_op jit(solution)/shard_map/reshape;transpose;transpose;reshape;reshape;reshape | solution.py:86
  198.6 37.4 %all_to_all.23 = bf16[128,1,1,4,2048]{4,3,2,1,0:T(4,128)(2,1)} all-to-all(bf16[128,1,1,4,2048]{4,3,2,1,0:T(4,128)(2,1)} %reshape_transpose_transpose_reshape_reshape_reshape.6), channel_id=1, replica_groups=mesh['sp_0'=4,'sp_1'=4,'sp_2'=4,'tp'=2] {'sp_0','sp_1','sp_2','tp'}, dimensions={0} | all-to-all | bytes 4194304 | tf_op jit(solution)/shard_map/all_to_all | solution.py:87
  235.9 4.0 %reshape_reshape.6 = bf16[512,2048]{1,0:T(8,128)(2,1)} reshape(bf16[64,2,1,4,2048]{4,3,1,0,2:T(4,128)(2,1)} %bitcast.338) | data formatting | bytes 4194304 | tf_op jit(solution)/shard_map/reshape;reshape | solution.py:281
  239.9 4.4 %fusion.45 = f32[512,512]{1,0:T(8,128)} fusion(bf16[512,2048]{1,0:T(8,128)(2,1)} %reshape_reshape.6, bf16[1,2048,512]{2,1,0:T(8,128)(2,1)} %param.43), kind=kOutput, calls=%fused_computation.60 | convolution fusion | flops 1073741824 | bytes 5242880 | tf_op jit(solution)/shard_map/dot_general | solution.py:282
  244.3 6.2 %convolution_convert_fusion = bf16[512,2048]{1,0:T(8,128)(2,1)} fusion(bf16[1,512,2048]{2,1,0:T(8,128)(2,1)S(1)} %copy-done, bf16[512,2048]{1,0:T(8,128)(2,1)} %reshape_reshape.6, bf16[1,2048,512]{2,1,0:T(8,128)(2,1)} %param.44, f32[512,512]{1,0:T(8,128)} %fusion.45), kind=kOutput, calls=%fused_computation.55 | convolution fusion | flops 2150105088 | bytes 9437184 | tf_op jit(solution)/shard_map/dot_general | solution.py:286
  250.6 4.1 %reshape_transpose_transpose_reshape_reshape_reshape.7 = bf16[128,1,1,4,2048]{4,3,0,2,1:T(4,128)(2,1)} reshape(bf16[512,2048]{1,0:T(8,128)(2,1)} %convolution_convert_fusion) | data formatting | bytes 4194304 | tf_op jit(solution)/shard_map/reshape;transpose;transpose;reshape;reshape;reshape | solution.py:86
  254.7 5.8 %all-to-all-start.3 = ((bf16[128,1,1,4,2048]{4,3,2,1,0:T(4,128)(2,1)}), bf16[128,1,1,4,2048]{4,3,2,1,0:T(4,128)(2,1)}, u32[]{:S(2)}, u32[]{:S(2)}) async-start(bf16[128,1,1,4,2048]{4,3,2,1,0:T(4,128)(2,1)} %bitcast.337), calls=%async_computation.3 | async-start | bytes 4194304 | tf_op jit(solution)/shard_map/all_to_all | solution.py:87
  260.7 30.1 %all-to-all-done.3 = bf16[128,1,1,4,2048]{4,3,2,1,0:T(4,128)(2,1)} async-done(((bf16[128,1,1,4,2048]{4,3,2,1,0:T(4,128)(2,1)}), bf16[128,1,1,4,2048]{4,3,2,1,0:T(4,128)(2,1)}, u32[]{:S(2)}, u32[]{:S(2)}) %all-to-all-start.3) | async-done | bytes 2097184 | tf_op jit(solution)/shard_map/all_to_all | solution.py:87
  290.7 4.0 %reshape_reshape.7 = bf16[512,2048]{1,0:T(8,128)(2,1)} reshape(bf16[64,2,1,4,2048]{4,3,1,0,2:T(4,128)(2,1)} %bitcast.90) | data formatting | bytes 4194304 | tf_op jit(solution)/shard_map/reshape;reshape | solution.py:291
  294.7 5.2 %gather_fusion = bf16[256,2048]{1,0:T(8,128)(2,1)} fusion(bf16[512,2048]{1,0:T(8,128)(2,1)} %reshape_reshape.7, s32[1024]{0:T(1024)S(1)} %pad_clamp_fusion), kind=kCustom, calls=%fused_computation.1 | custom fusion | bytes 2098176 | tf_op jit(solution)/shard_map/gather | solution.py:291
  299.9 3.4 %reshape.960 = f32[128,2,2048]{2,1,0:T(2,128)} reshape(bf16[256,2048]{1,0:T(8,128)(2,1)} %gather_fusion) | data formatting | bytes 3145728 | tf_op jit(solution)/shard_map/convert_element_type | solution.py:303
  303.3 4.8 %multiply_reduce_fusion = f32[128,2048]{1,0:T(8,128)S(1)} fusion(f32[128,2,2048]{2,1,0:T(2,128)} %reshape.960, f32[128,2]{1,0:T(8,128)S(1)} %copy.128), kind=kLoop, calls=%fused_computation.62 | loop fusion | flops 786432 | bytes 3146752 | tf_op jit(solution)/shard_map/reduce_sum | solution.py:302
  308.1 0.9 fusion.66
  (137 shorter events, 23.4 us)
Async XLA Ops:
  6.5 237.8 %copy-start = (bf16[1,512,2048]{2,1,0:T(8,128)(2,1)S(1)}, bf16[1,512,2048]{2,1,0:T(8,128)(2,1)}, u32[]{:S(2)}) copy-start(bf16[1,512,2048]{2,1,0:T(8,128)(2,1)} %param.45) | copy-start | bytes 6291460
  6.5 24.7 %copy-start.1 = (bf16[256,1024]{1,0:T(8,128)(2,1)S(1)}, bf16[256,1024]{1,0:T(8,128)(2,1)}, u32[]{:S(2)}) copy-start(bf16[256,1024]{1,0:T(8,128)(2,1)} %param.24) | copy-start | bytes 1572868
  6.5 100.2 %all-gather.10.cloned.1.call-start = ((), (), s32[]{:S(2)}) async-start(), calls=%async_computation.6 | async-start | bytes 1310720 | tf_op jit(solution)/shard_map/all_gather | solution.py:37
  7.5 17.4 %collective-permute-start = (bf16[3]{0:T(256)(128)(2,1)S(1)}, bf16[3]{0:T(256)(128)(2,1)S(1)}, u32[]{:S(2)}, u32[]{:S(2)}) collective-permute-start(bf16[3]{0:T(256)(128)(2,1)S(1)} %slice.237), channel_id=1, source_target_pairs={{0,2},{2,4},{4,6},{6,8},{8,10},{10,12},{12,14},{14,16},{16,18},{18... | collective-permute-start | bytes 26 | tf_op jit(solution)/shard_map/ppermute | solution.py:22
  12.1 19.1 %collective-permute-start.1 = (bf16[3,1024]{1,0:T(4,128)(2,1)S(1)}, bf16[3,1024]{1,0:T(4,128)(2,1)S(1)}, u32[]{:S(2)}, u32[]{:S(2)}) collective-permute-start(bf16[3,1024]{1,0:T(4,128)(2,1)S(1)} %slice.240), channel_id=1, source_target_pairs={{0,2},{2,4},{4,6},{6,8},{8,10},{10,12},{12,14},{14,16},{16,18},{18... | collective-permute-start | bytes 18440 | tf_op jit(solution)/shard_map/ppermute | solution.py:22
  15.9 13.3 %collective-permute-start.3 = (bf16[3,128]{1,0:T(4,128)(2,1)S(1)}, bf16[3,128]{1,0:T(4,128)(2,1)S(1)}, u32[]{:S(2)}, u32[]{:S(2)}) collective-permute-start(bf16[3,128]{1,0:T(4,128)(2,1)S(1)} %slice.261), channel_id=1, source_target_pairs={{0,2},{2,4},{4,6},{6,8},{8,10},{10,12},{12,14},{14,16},{16,18},{18... | collective-permute-start | bytes 2312 | tf_op jit(solution)/shard_map/ppermute | solution.py:22
  19.4 10.7 %collective-permute-start.2 = (bf16[3,128]{1,0:T(4,128)(2,1)S(1)}, bf16[3,128]{1,0:T(4,128)(2,1)S(1)}, u32[]{:S(2)}, u32[]{:S(2)}) collective-permute-start(bf16[3,128]{1,0:T(4,128)(2,1)S(1)} %slice.252), channel_id=1, source_target_pairs={{0,2},{2,4},{4,6},{6,8},{8,10},{10,12},{12,14},{14,16},{16,18},{18... | collective-permute-start | bytes 2312 | tf_op jit(solution)/shard_map/ppermute | solution.py:22
  41.2 40.3 %copy-start.11 = (u32[128]{0:T(128)S(1)}, u32[128]{0:T(128)}, u32[]{:S(2)}) copy-start(u32[128]{0:T(128)} %constant.133) | copy-start | bytes 1540
  80.6 28.5 %copy-start.5 = (s32[128,2]{0,1:T(2,128)S(1)}, s32[128,2]{0,1:T(2,128)}, u32[]{:S(2)}) copy-start(s32[128,2]{0,1:T(2,128)} %param.42) | copy-start | bytes 3076
  80.6 29.1 %copy-start.10 = (u32[128]{0:T(128)S(1)}, u32[128]{0:T(128)}, u32[]{:S(2)}) copy-start(u32[128]{0:T(128)} %constant.143) | copy-start | bytes 1540
  81.4 52.3 %all-gather.6.cloned.1.call-start = ((), (), s32[]{:S(2)}) async-start(), calls=%async_computation.4 | async-start | bytes 1310720 | tf_op jit(solution)/shard_map/all_gather | solution.py:37
  106.7 29.6 %copy-start.9 = (u32[128]{0:T(128)S(1)}, u32[128]{0:T(128)}, u32[]{:S(2)}) copy-start(u32[128]{0:T(128)} %constant.148) | copy-start | bytes 1540
  109.0 51.7 %all-gather.8.cloned.1.call-start = ((), (), s32[]{:S(2)}) async-start(), calls=%async_computation.5 | async-start | bytes 1310720 | tf_op jit(solution)/shard_map/all_gather | solution.py:37
  133.6 27.1 %copy-start.8 = (f32[16]{0:T(128)S(1)}, f32[16]{0:T(128)}, u32[]{:S(2)}) copy-start(f32[16]{0:T(128)} %param.31) | copy-start | bytes 196
  165.4 2.6 copy-start.3
  165.4 12.9 %dynamic-slice-start = ((f32[2048]{0:T(1024)}, s32[]{:T(128)}), f32[1024]{0:T(1024)S(1)}, s32[]{:S(2)}) async-start(f32[2048]{0:T(1024)} %param.36, s32[]{:T(128)} %select_n.371), calls=%async_computation.7 | async-start | bytes 8704 | tf_op jit(solution)/shard_map/dynamic_slice | solution.py:255
  181.9 4.9 %copy-start.2 = (bf16[128,2048]{1,0:T(8,128)(2,1)S(1)}, bf16[128,2048]{1,0:T(8,128)(2,1)}, u32[]{:S(2)}) copy-start(bf16[128,2048]{1,0:T(8,128)(2,1)} %param.37) | copy-start | bytes 1572868
  186.6 0.7 copy-start.4
  254.7 5.8 %copy-start.6 = (f32[128,4]{0,1:T(4,128)S(1)}, f32[128,4]{0,1:T(4,128)}, u32[]{:S(2)}) copy-start(f32[128,4]{0,1:T(4,128)} %param.40) | copy-start | bytes 6148
  254.7 5.9 %copy-start.7 = (f32[128,2]{0,1:T(2,128)S(1)}, f32[128,2]{0,1:T(2,128)}, u32[]{:S(2)}) copy-start(f32[128,2]{0,1:T(2,128)} %param.41) | copy-start | bytes 3076
  254.7 36.1 %all-to-all-start.3 = ((bf16[128,1,1,4,2048]{4,3,2,1,0:T(4,128)(2,1)}), bf16[128,1,1,4,2048]{4,3,2,1,0:T(4,128)(2,1)}, u32[]{:S(2)}, u32[]{:S(2)}) async-start(bf16[128,1,1,4,2048]{4,3,2,1,0:T(4,128)(2,1)} %bitcast.337), calls=%async_computation.3 | async-start | bytes 4194304 | tf_op jit(solution)/shard_map/all_to_all | solution.py:87
Sparse Core Ops, SparseCore 0:
  81.5 25.1 all-gather.9
  109.1 24.4 all-gather.5
  136.0 24.6 all-gather.7
where the time goes:
time: 319 us; the launch traced here: 316 us
  blocking collectives  86.7 us (27%)
  local copies, waits for them, and re-layouts  82.2 us (26%)
  waiting for transfers between devices  43.1 us (14%)
  between operations  28.2 us (9%)
  other arithmetic  27.6 us (9%)
  matrix products  26.7 us (8%)
  starting transfers between devices  18.8 us (6%)
    all_to_all x1, blocking collectives, joined_exchange(): tiles = lax.all_to_all(tiles, axis, split_axis=0, concat_axis=0, tiled=True)  37.4 us
    all_to_all x1, waiting for transfers between devices, joined_exchange(): tiles = lax.all_to_all(tiles, axis, split_axis=0, concat_axis=0, tiled=True)  30.1 us
    dynamic_update_slice x2, local copies, waits for them, and re-layouts, local(): lax.scan(block_step, initial, (step_values.reshape(blocks, BLOCK, groups,...  26.1 us
    unnamed x3, blocking collectives  25.5 us
    all_gather x3, waiting for transfers between devices, carried_in_2(): lax.all_gather(part.astype(kind), axis)  13 us
    ppermute x4, starting transfers between devices, shifted(): return lax.ppermute(block, axis, route)  12.9 us
    all_gather x2, blocking collectives, carried_in_2(): lax.all_gather(part.astype(kind), axis)  10.5 us
    all_to_all x1, blocking collectives, copy_for_each(): lax.all_to_all(jnp.broadcast_to(array[None], (count, *array.shape)), axis...  8.65 us
  transfers between devices with their start and end apart: 8, of which 4 were waited for; matrix products, arithmetic and copies ran while one was open for 7% of the time, Pallas kernels for 0%

commit v1 on v0

v1 whole, which is shorter than its diff:
```python
import functools

import jax
import jax.numpy as jnp
from jax import lax
from jax.experimental import pallas as pl
from jax.experimental.pallas import tpu as pltpu
from jax.sharding import Mesh
from jax.sharding import PartitionSpec as P

SP = ("sp_0", "sp_1", "sp_2")
SP_TP = ("sp_0", "sp_1", "sp_2", "tp")
ROW = "sp_2"

EPS = 1e-06
LEN = 256
BLK = 128
CH = 1024
HEADS = 16
HD = 64
NS = 128
D = 2048
EXPERTS = 128
CAP = 4
QW = 512
HID = 512
SLOTS = EXPERTS * CAP
PAY = 136
NEG = -1e30
F32 = jnp.float32
BF16 = jnp.bfloat16
HIGH = lax.Precision.HIGHEST


def vmem(n):
    return [pl.BlockSpec(memory_space=pltpu.VMEM)] * n


def call(body, outs, n_in, scratch=(), limit=32, cost=None, in_specs=None, name=None):
    return pl.pallas_call(
        body,
        out_shape=outs,
        in_specs=in_specs or vmem(n_in),
        out_specs=jax.tree.map(lambda _: pl.BlockSpec(memory_space=pltpu.VMEM), outs),
        scratch_shapes=list(scratch),
        compiler_params=pltpu.CompilerParams(vmem_limit_bytes=limit * 1024 * 1024),
        cost_estimate=cost,
        name=name,
    )


def sds(shape, dtype):
    return jax.ShapeDtypeStruct(shape, dtype)


def iota(shape, dim):
    return lax.broadcasted_iota(jnp.int32, shape, dim)


def mm(a, b, precision=None):
    return jnp.dot(a, b, preferred_element_type=F32, precision=precision)


def softplus(v):
    return jnp.maximum(v, 0.0) + jnp.log(1.0 + jnp.exp(-jnp.abs(v)))


def silu(v):
    return v / (1.0 + jnp.exp(-v))


def head_expand():
    return (iota((HEADS, CH), 1) // HD == iota((HEADS, CH), 0)).astype(F32)


def split2(v):
    hi = v.astype(BF16)
    return hi, (v - hi.astype(F32)).astype(BF16)


def logs(step_ref, extra_ref, rate_ref):
    step = softplus(step_ref[...])
    return step, extra_ref[...] - step * rate_ref[...]


def cumulated(logd):
    tri = (iota((LEN, LEN), 0) >= iota((LEN, LEN), 1)).astype(F32)
    return mm(tri, logd, HIGH)


def conv(pad_ref, taps, masks, lo, width):
    acc = pad_ref[8 : 8 + LEN, lo : lo + width] * taps[3:4, lo : lo + width]
    for k in range(3):
        term = pad_ref[5 + k : 5 + k + LEN, lo : lo + width] * taps[k : k + 1, lo : lo + width]
        acc = acc + term * masks[k][:, :1]
    return silu(acc).astype(BF16)


def conv_kernel(
    values, bmap, cmap, edges, docs, step_pre, extra, rate, vtaps, btaps, ctaps,
    pay, xs_out, vc_out, bc_out, cc_out,
    vpad, mpad, dpad,
):
    vpad[0:8, :] = edges[:, 0:CH].astype(F32)
    vpad[8:, :] = values[...].astype(F32)
    mpad[0:8, :] = edges[:, CH : CH + 2 * NS].astype(F32)
    mpad[8:, 0:NS] = bmap[...].astype(F32)
    mpad[8:, NS:] = cmap[...].astype(F32)
    dpad[0:8, :] = edges[:, CH + 2 * NS :].astype(F32)
    dpad[8:, :] = docs[...]
    own = dpad[8:, :]
    masks = [(dpad[5 + k : 5 + k + LEN, :] == own).astype(F32) for k in range(3)]
    step, logd = logs(step_pre, extra, rate)
    cum = cumulated(logd)
    total = cum[LEN - 1 : LEN, :]
    last = dpad[8 + LEN - 1 : 8 + LEN, :]
    tail = (own == last).astype(F32)
    weight = jnp.exp(total - cum) * tail[:, :HEADS]
    expand = head_expand()
    step_x = mm(step, expand, HIGH)
    weight_x = mm(weight, expand, HIGH)
    taps_b = btaps[...].astype(F32)
    taps_c = ctaps[...].astype(F32)
    taps_m = jnp.concatenate([taps_b, taps_c], axis=1)
    both = conv(mpad, taps_m, masks, 0, 2 * NS)
    bc = both[:, 0:NS]
    bc_out[...] = bc
    cc_out[...] = both[:, NS:]
    bt = jnp.transpose(bc.astype(F32)).astype(BF16)
    taps_v = vtaps[...].astype(F32)
    passing = (last == dpad[7:8, :]).astype(F32)
    factor = mm(jnp.exp(total) * passing[:, :HEADS], expand, HIGH)
    for q in range(4):
        lo = q * 256
        vc = conv(vpad, taps_v, masks, lo, 256)
        vc_out[:, lo : lo + 256] = vc
        xs = (step_x[:, lo : lo + 256] * vc.astype(F32)).astype(BF16)
        xs_out[:, lo : lo + 256] = xs
        ev = (weight_x[:, lo : lo + 256] * xs.astype(F32)).astype(BF16)
        pay[q, 0:NS, :] = mm(bt, ev).astype(BF16)
        hi, low = split2(factor[:, lo : lo + 256])
        rows = iota((8, 256), 0)
        pay[q, NS:PAY, :] = jnp.where(
            rows == 0, hi.astype(F32), jnp.where(rows == 1, low.astype(F32), 0.0)
        ).astype(BF16)


def row_prefix(got):
    states = [got[x, 0:NS, :].astype(F32) for x in range(4)]
    factors = [
        got[x, NS:PAY, :].astype(F32)[0:1] + got[x, NS:PAY, :].astype(F32)[1:2] for x in range(4)
    ]
    before = [None]
    passed = [jnp.ones_like(factors[0])]
    run, gain = states[0], factors[0]
    for x in range(1, 4):
        before.append(run)
        passed.append(gain)
        run = states[x] + factors[x] * run
        gain = factors[x] * gain
    return before, passed, run, gain


def row_total_kernel(got, out):
    _, _, run, gain = row_prefix(got)
    out[0:NS, :] = run.astype(BF16)
    hi, low = split2(gain)
    rows = iota((8, 256), 0)
    out[NS:PAY, :] = jnp.where(
        rows == 0, hi.astype(F32), jnp.where(rows == 1, low.astype(F32), 0.0)
    ).astype(BF16)


def row_carry_kernel(got, one, two, out):
    before, passed, _, _ = row_prefix(got)
    tail = one[NS:PAY, :].astype(F32)
    carry = one[0:NS, :].astype(F32) + (tail[0:1] + tail[1:2]) * two[0:NS, :].astype(F32)
    out[0] = carry.astype(BF16)
    for x in range(1, 4):
        out[x] = (before[x] + passed[x] * carry).astype(BF16)


def inner_kernel(
    xs, vc, bc, cc, docs, docs_row, edges, step_pre, extra, rate, direct, gate,
    p_out, g_out,
    lpad, cum_t,
):
    _, logd = logs(step_pre, extra, rate)
    lpad[...] = jnp.zeros_like(lpad)
    lpad[:, 0:HEADS] = logd
    cum = cumulated(lpad[...])
    cum_t[...] = jnp.transpose(cum)
    expand = head_expand()
    own = docs[...]
    prev = edges[:, CH + 2 * NS :].astype(F32)[7:8, :]
    enter = jnp.exp(cum[:, :HEADS]) * (own == prev).astype(F32)[:, :HEADS]
    enter_x = mm(enter, expand, HIGH)
    mid = cum[BLK - 1 : BLK, :HEADS]
    mid_doc = own[BLK - 1 : BLK, :]
    w0 = jnp.exp(mid - cum[0:BLK, :HEADS]) * (own[0:BLK, :HEADS] == mid_doc[:, :HEADS]).astype(F32)
    w0_x = mm(w0, expand, HIGH)
    r1 = jnp.exp(cum[BLK:, :HEADS] - mid) * (own[BLK:, :HEADS] == mid_doc[:, :HEADS]).astype(F32)
    r1_x = mm(r1, expand, HIGH)
    ev0 = (w0_x * xs[0:BLK, :].astype(F32)).astype(BF16)
    bt0 = jnp.transpose(bc[0:BLK, :].astype(F32)).astype(BF16)
    state0 = mm(bt0, ev0).astype(BF16)
    direct_x = mm(direct[...], expand, HIGH)
    lane = iota((BLK, 2 * HD), 1)
    for b in range(2):
        rows = slice(b * BLK, (b + 1) * BLK)
        cb = cc[rows, :]
        scores = lax.dot_general(
            cb, bc[rows, :], (((1,), (1,)), ((), ())), preferred_element_type=F32
        )
        allowed = (iota((BLK, BLK), 0) >= iota((BLK, BLK), 1)) & (
            own[rows, :] == docs_row[b : b + 1, :]
        )
        bias = jnp.where(allowed, 0.0, NEG)
        for j in range(CH // (2 * HD)):
            cols = slice(j * 128, (j + 1) * 128)
            chunk = xs[rows, cols]
            parts = []
            for h in (2 * j, 2 * j + 1):
                spread = cum[rows, h : h + 1] - cum_t[h : h + 1, rows]
                weighted = (scores * jnp.exp(spread + bias)).astype(BF16)
                parts.append(mm(weighted, chunk))
            y = jnp.where(lane < HD, parts[0], parts[1])
            if b == 1:
                y = y + mm(cb, state0[:, cols]) * r1_x[:, cols]
            y = y + vc[rows, cols].astype(F32) * direct_x[:, cols]
            act = silu(gate[rows, cols].astype(F32))
            p_out[rows, cols] = y * act
            g_out[rows, cols] = act * enter_x[rows, cols]


def outer_kernel(cc, state, p, g, keep, send):
    core = lax.axis_index("tp")

    def half(b, out):
        rows = slice(b * BLK, (b + 1) * BLK)
        for q in range(4):
            cols = slice(q * 256, (q + 1) * 256)
            read = mm(cc[rows, :], state[q])
            out[:, cols] = (p[rows, cols] + g[rows, cols] * read).astype(BF16)

    @pl.when(core == 0)
    def _():
        half(0, keep)
        half(1, send)

    @pl.when(core == 1)
    def _():
        half(1, keep)
        half(0, send)


def route_kernel(chosen, chosen_w, group_w, col_out, row_out):
    lanes = iota((128, EXPERTS), 1)
    hot = [(chosen[:, k : k + 1] == lanes).astype(F32) for k in range(2)]
    below = (iota((128, 128), 0) > iota((128, 128), 1)).astype(BF16)
    rank = mm(below, (hot[0] + hot[1]).astype(BF16))
    out = jnp.zeros((128, 128), F32)
    for k in range(2):
        index = chosen[:, k : k + 1]
        slot = index.astype(F32) * CAP + jnp.sum(rank * hot[k], axis=1, keepdims=True)
        weight = jnp.zeros((128, 1), F32)
        for g in range(4):
            weight = weight + jnp.where((index >> 5) == g, group_w[:, g : g + 1], 0.0)
        weight = weight * chosen_w[:, k : k + 1]
        out = jnp.where(lanes == k, slot, out)
        out = jnp.where(lanes == 2 + k, weight, out)
    col_out[...] = out
    row_out[...] = jnp.transpose(out)[0:8, :]


def unpack_matrix():
    out = iota((256, 256), 0)
    r = iota((256, 256), 1)
    return (out == ((r >> 2) & 3) * 64 + (r >> 4) * 4 + (r & 3)).astype(BF16)


def pack_matrix():
    r = iota((256, 256), 0)
    src = iota((256, 256), 1)
    return (src == ((r >> 2) & 3) * 64 + (r >> 4) * 4 + (r & 3)).astype(BF16)


def proj_kernel(
    keep, got, w_hbm, gain, residual, gain2, route,
    mixed_out, out,
    w, ybuf, sem,
):
    core = lax.axis_index("tp")
    order = [core, 1 - core]
    copies = []
    for i in range(4):
        start = pl.multiple_of(order[i // 2] * CH + (i % 2) * 512, 512)
        copy = pltpu.make_async_copy(
            w_hbm.at[pl.ds(start, 512), :], w.at[pl.ds(i * 512, 512), :], sem.at[i]
        )
        copy.start()
        copies.append(copy)
    a = keep[...].astype(F32)
    b = got[...].astype(F32)
    squares = jnp.sum(a * a, axis=1, keepdims=True) + jnp.sum(b * b, axis=1, keepdims=True)
    factor = lax.rsqrt(squares * (1.0 / D) + EPS)
    ga = gain[pl.ds(core, 1), :]
    gb = gain[pl.ds(1 - core, 1), :]
    na = (a * factor * ga).astype(BF16)
    nb = (b * factor * gb).astype(BF16)
    total = residual[...].astype(F32)
    for i in range(4):
        part = (na, nb)[i // 2][:, (i % 2) * 512 : (i % 2 + 1) * 512]
        copies[i].wait()
        total = total + mm(part, w[i * 512 : (i + 1) * 512, :])
    mixed = total.astype(BF16)
    mixed_out[...] = mixed
    wide = mixed.astype(F32)
    mean = jnp.sum(wide * wide, axis=1, keepdims=True) * (1.0 / D)
    rows_in = (wide * lax.rsqrt(mean + EPS) * gain2[...]).astype(BF16)
    slots = iota((SLOTS, 128), 0).astype(F32)
    hot = (slots == route[0:1, :]) | (slots == route[1:2, :])
    ybuf[...] = mm(hot.astype(BF16), rows_in).astype(BF16)
    pack = pack_matrix()
    for blk in range(8):
        rows = slice(blk * 64, (blk + 1) * 64)
        stacked = jnp.concatenate(
            [ybuf[rows, q * QW : (q + 1) * QW] for q in range(4)], axis=0
        )
        out[blk * 256 : (blk + 1) * 256, :] = mm(pack, stacked).astype(BF16)


def expert_kernel(
    arrived, gate_hbm, up_hbm, down_hbm,
    out,
    wg, wu, wd, x, sem,
):
    copies = [
        pltpu.make_async_copy(src.at[0], dst, sem.at[i])
        for i, (src, dst) in enumerate(((gate_hbm, wg), (up_hbm, wu), (down_hbm, wd)))
    ]
    for copy in copies:
        copy.start()
    unpack = unpack_matrix()
    for blk in range(8):
        flat = mm(unpack, arrived[blk * 256 : (blk + 1) * 256, :]).astype(BF16)
        for q in range(4):
            x[blk * 64 : (blk + 1) * 64, q * QW : (q + 1) * QW] = flat[q * 64 : (q + 1) * 64, :]
    for copy in copies:
        copy.wait()
    pack = pack_matrix()
    for half in range(2):
        rows = slice(half * 256, (half + 1) * 256)
        g = mm(x[rows, :], wg[...])
        u = mm(x[rows, :], wu[...])
        hidden = (silu(g) * u).astype(BF16)
        y = mm(hidden, wd[...]).astype(BF16)
        for i in range(4):
            stacked = jnp.concatenate(
                [y[i * 64 : (i + 1) * 64, q * QW : (q + 1) * QW] for q in range(4)], axis=0
            )
            blk = half * 4 + i
            out[blk * 256 : (blk + 1) * 256, :] = mm(pack, stacked).astype(BF16)


def combine_kernel(back, mixed, route, out, r):
    unpack = unpack_matrix()
    for blk in range(8):
        flat = mm(unpack, back[blk * 256 : (blk + 1) * 256, :]).astype(BF16)
        for q in range(4):
            r[blk * 64 : (blk + 1) * 64, q * QW : (q + 1) * QW] = flat[q * 64 : (q + 1) * 64, :]
    slots = iota((128, SLOTS), 1).astype(F32)
    info = route[...]
    q_mat = jnp.where(slots == info[:, 0:1], info[:, 2:3], 0.0) + jnp.where(
        slots == info[:, 1:2], info[:, 3:4], 0.0
    )
    hi, low = split2(q_mat)
    for q in range(4):
        cols = slice(q * QW, (q + 1) * QW)
        acc = mm(hi, r[:, cols]) + mm(low, r[:, cols])
        out[:, cols] = (mixed[:, cols].astype(F32) + acc).astype(BF16)


def shifted(block, distance):
    count = 1
    for axis in SP:
        count *= lax.axis_size(axis)
    return lax.ppermute(block, SP, [(i, i + distance) for i in range(count - distance)])


def local(
    mixer_value_rows,
    input_map_rows,
    output_map_rows,
    gate_preactivation,
    step_preactivation,
    position_extra_decay,
    head_decay_rate,
    head_direct_term,
    value_taps,
    input_map_taps,
    output_map_taps,
    document_index,
    gated_norm_gain,
    residual,
    mixer_output_weight,
    expert_norm_gain,
    expert_group_weight,
    chosen_expert_weight,
    chosen_expert_index,
    expert_gate_weight,
    expert_up_weight,
    expert_down_weight,
):
    marks = (document_index + 1).astype(F32)
    docs = jnp.broadcast_to(marks[:, None], (LEN, 128))
    docs_row = marks.reshape(2, 128)
    edge = jnp.concatenate(
        [
            mixer_value_rows[-8:],
            input_map_rows[-8:],
            output_map_rows[-8:],
            docs[-8:].astype(BF16),
        ],
        axis=1,
    )
    edges = shifted(edge, 1)
    rate = head_decay_rate.reshape(1, HEADS)
    direct = head_direct_term.reshape(1, HEADS)
    route_col, route_row = call(
        route_kernel, (sds((128, 128), F32), sds((8, 128), F32)), 3, name="route"
    )(chosen_expert_index, chosen_expert_weight, expert_group_weight)
    pay, xs, vc, bc, cc = call(
        conv_kernel,
        (
            sds((4, PAY, 256), BF16),
            sds((LEN, CH), BF16),
            sds((LEN, CH), BF16),
            sds((LEN, NS), BF16),
            sds((LEN, NS), BF16),
        ),
        11,
        scratch=(
            pltpu.VMEM((LEN + 8, CH), F32),
            pltpu.VMEM((LEN + 8, 2 * NS), F32),
            pltpu.VMEM((LEN + 8, 128), F32),
        ),
        name="conv",
    )(
        mixer_value_rows, input_map_rows, output_map_rows, edges, docs,
        step_preactivation, position_extra_decay, rate,
        value_taps, input_map_taps, output_map_taps,
    )
    got = lax.all_to_all(pay, ROW, 0, 0, tiled=True)
    total = call(row_total_kernel, sds((PAY, 256), BF16), 1, name="row_total")(got)
    one, two = shifted(total, 4), shifted(total, 8)
    p, g = call(
        inner_kernel,
        (sds((LEN, CH), F32), sds((LEN, CH), F32)),
        12,
        scratch=(pltpu.VMEM((LEN, 128), F32), pltpu.VMEM((128, LEN), F32)),
        cost=pl.CostEstimate(flops=4_000_000_000, bytes_accessed=4_000_000, transcendentals=0),
        name="inner",
    )(
        xs, vc, bc, cc, docs, docs_row, edges, step_preactivation, position_extra_decay,
        rate, direct, gate_preactivation,
    )
    carried = call(row_carry_kernel, sds((4, NS, 256), BF16), 3, name="row_carry")(got, one, two)
    state = lax.all_to_all(carried, ROW, 0, 0, tiled=True)
    keep, send = call(
        outer_kernel, (sds((BLK, CH), BF16), sds((BLK, CH), BF16)), 4, name="outer"
    )(cc, state, p, g)
    other = lax.ppermute(send, "tp", [(0, 1), (1, 0)])
    mixed, outgoing = call(
        proj_kernel,
        (sds((128, D), BF16), sds((EXPERTS * 16, QW), BF16)),
        7,
        scratch=(
            pltpu.VMEM((D, D), BF16),
            pltpu.VMEM((SLOTS, D), BF16),
            pltpu.SemaphoreType.DMA((4,)),
        ),
        in_specs=vmem(2) + [pl.BlockSpec(memory_space=pl.ANY)] + vmem(4),
        name="proj",
    )(
        keep, other, mixer_output_weight, gated_norm_gain.reshape(2, CH), residual,
        expert_norm_gain.reshape(1, D), route_row,
    )
    arrived = lax.all_to_all(outgoing.reshape(EXPERTS, 16, QW), SP_TP, 0, 0, tiled=True)
    finished = call(
        expert_kernel,
        sds((EXPERTS * 16, QW), BF16),
        4,
        scratch=(
            pltpu.VMEM((D, HID), BF16),
            pltpu.VMEM((D, HID), BF16),
            pltpu.VMEM((HID, D), BF16),
            pltpu.VMEM((SLOTS, D), BF16),
            pltpu.SemaphoreType.DMA((3,)),
        ),
        in_specs=vmem(1) + [pl.BlockSpec(memory_space=pl.ANY)] * 3,
        name="expert",
    )(arrived.reshape(EXPERTS * 16, QW), expert_gate_weight, expert_up_weight, expert_down_weight)
    returned = lax.all_to_all(finished.reshape(EXPERTS, 16, QW), SP_TP, 0, 0, tiled=True)
    return call(
        combine_kernel,
        sds((128, D), BF16),
        3,
        scratch=(pltpu.VMEM((SLOTS, D), BF16),),
        name="combine",
    )(returned.reshape(EXPERTS * 16, QW), mixed, route_col)


def solution(mesh):
    torus = Mesh(mesh.devices.reshape(4, 4, 4, mesh.shape["tp"]), ("sp_0", "sp_1", "sp_2", "tp"))
    in_specs = (
        P(SP, "tp"),
        P(SP, "tp"),
        P(SP, "tp"),
        P(SP, "tp"),
        P(SP, "tp"),
        P(SP, "tp"),
        P("tp"),
        P("tp"),
        P(None, "tp"),
        P(None, "tp"),
        P(None, "tp"),
        P(SP),
        P(),
        P(SP_TP, None),
        P(),
        P(),
        P(SP_TP, None),
        P(SP_TP, None),
        P(SP_TP, None),
        P(SP_TP, None, None),
        P(SP_TP, None, None),
        P(SP_TP, None, None),
    )
    out_specs = P(SP_TP, None)
    return jax.shard_map(local, mesh=torus, in_specs=in_specs, out_specs=out_specs, check_vma=False)
```

time: 319 us -> 145 us (0.45)
  local copies, waits for them, and re-layouts: 82.2 us -> 17.1 us
  waiting for transfers between devices: 43.1 us -> 1.63 us
  between operations: 28.2 us -> 0.24 us
  other arithmetic: 27.6 us -> 0.69 us
  matrix products: 26.7 us -> 0 us
  Pallas kernels: 0 us -> 19 us
    all_to_all x3, blocking collectives: 50.7 us -> 86.5 us  [the longest x1 42.9 us: local(): lax.all_to_all(outgoing.reshape(EXPERTS, 16, QW), SP_TP, 0, 0, tiled=True)]
    all_to_all x1, waiting for transfers between devices: 30.1 us -> 0.01 us  [local(): state = lax.all_to_all(carried, ROW, 0, 0, tiled=True)]
    dot_general x12 -> x0, matrix products: 26.7 us -> none  [the longest x1 6.22 us: local(): jnp.dot(hidden, expert_down_weight[0], preferred_element_type=jnp.float32)]
    dynamic_update_slice x2 -> x0, local copies, waits for them, and re-layouts: 26.1 us -> none  [local(): lax.scan(block_step, initial, (step_values.reshape(blocks, BLOCK, groups,...]
    unnamed x3 -> x0, blocking collectives: 25.5 us -> none
    pallas_call x0 -> x9, Pallas kernels: none -> 19 us  [the longest x1 5.48 us: local(): call(expert_kernel, sds((EXPERTS * 16, QW), BF16), 4, scratch=(pltpu.VMEM...]
    another operation x10 -> x0, local copies, waits for them, and re-layouts: 16.3 us -> none  [the longest x2 8.22 us: joined_exchange(): tiles = tiles.reshape(-1, *inside)]
    convert_element_type x17 -> x0, other arithmetic: 15.1 us -> none  [the longest x3 5.25 us: carried_in_2(): part.astype(kind)]
  transfers between devices with their start and end apart: 8 -> 5, of which waited for: 4 -> 2; matrix products, arithmetic and copies ran while one was open for 7% -> 1% of each run, Pallas kernels for 0% -> 3%
where the time goes in v1:
time: 145 us; the launch traced here: 144 us
  blocking collectives  86.5 us (60%)
  starting transfers between devices  19.3 us (13%)
  Pallas kernels  19 us (13%)
  local copies, waits for them, and re-layouts  17.1 us (12%)
  waiting for transfers between devices  1.63 us (1%)
    all_to_all x1, blocking collectives, local(): lax.all_to_all(outgoing.reshape(EXPERTS, 16, QW), SP_TP, 0, 0, tiled=True)  42.9 us
    all_to_all x1, blocking collectives, local(): lax.all_to_all(finished.reshape(EXPERTS, 16, QW), SP_TP, 0, 0, tiled=True)  34.4 us
    unnamed x51, local copies, waits for them, and re-layouts  14.8 us
    ppermute x3, starting transfers between devices, shifted(): lax.ppermute(block, SP, [(i, i + distance) for i in range(count - distanc...  11.7 us
    all_to_all x1, blocking collectives, local(): got = lax.all_to_all(pay, ROW, 0, 0, tiled=True)  9.2 us
    pallas_call x1, Pallas kernels, local(): call(expert_kernel, sds((EXPERTS * 16, QW), BF16), 4, scratch=(pltpu.VMEM...  5.48 us
    ppermute x1, starting transfers between devices, local(): other = lax.ppermute(send, 'tp', [(0, 1), (1, 0)])  4.19 us
    pallas_call x1, Pallas kernels, local(): call(proj_kernel, (sds((128, D), BF16), sds((EXPERTS * 16, QW), BF16)), 7...  3.7 us
  transfers between devices with their start and end apart: 5, of which 2 were waited for; matrix products, arithmetic and copies ran while one was open for 1% of the time, Pallas kernels for 3%

profile of v1, /device:TPU:1, one launch (start us, length us, event | category | flops | bytes accessed | tf_op | source)
XLA Modules:
  0.0 144.5 jit_solution(10959247520483138591)
XLA Ops:
  0.0 0.7 slice.16
  0.7 0.7 slice.17
  1.4 0.7 fusion
  2.1 0.1 slice.18
  2.1 0.7 slice.15
  2.9 0.1 broadcast_in_dim.8
  2.9 3.9 %collective-permute-start = (bf16[8,1408]{1,0:T(8,128)(2,1)S(1)}, bf16[8,1408]{1,0:T(8,128)(2,1)S(1)}, u32[]{:S(2)}, u32[]{:S(2)}) collective-permute-start(bf16[8,1408]{1,0:T(8,128)(2,1)S(1)} %pad_maximum_fusion), channel_id=1, source_target_pairs={{0,2},{2,4},{4,6},{6,8},{8,10},{10,12},{12,14},{14,16},{16,18},{18... | collective-permute-start | bytes 67592 | tf_op jit(solution)/shard_map/ppermute | solution.py:388
  6.9 0.8 copy.23.step_pre
  7.7 0.8 copy.24.extra
  8.5 0.1 broadcast_in_dim.9.docs
  8.6 0.0 copy-start.4
  8.6 1.0 copy-done.4
  9.7 0.8 copy-done.6
  10.5 0.8 copy-done.7
  11.3 0.7 copy-done.8
  12.0 0.7 copy-done.10
  12.7 0.7 copy-done.11
  13.4 0.7 copy-done.12
  14.0 2.5 %conv.1 = (bf16[4,136,256]{2,1,0:T(8,128)(2,1)S(1)}, bf16[256,1024]{1,0:T(8,128)(2,1)S(1)}, bf16[256,1024]{1,0:T(8,128)(2,1)S(1)}, bf16[256,128]{1,0:T(8,128)(2,1)S(1)}, bf16[256,128]{1,0:T(8,128)(2,1)S(1)}) custom-call(bf16[256,1024]{1,0:T(8,128)(2,1)S(1)} %copy-done.4, bf16[256,128]{1,0:T(8,128)(2,1)S(1)} %copy-done.6, bf16[256,128]{1,0:T(8,128)(2,1)S(1)} %copy-done.7, ...), custom_call_target="tpu_custom_call" | custom-call | tf_op jit(solution)/shard_map/conv/pallas_call | solution.py:433
  16.6 0.8 copy-done.16
  17.4 9.2 %all_to_all.20.got = bf16[4,136,256]{2,1,0:T(8,128)(2,1)S(1)} all-to-all(bf16[4,136,256]{2,1,0:T(8,128)(2,1)S(1)} %get-tuple-element.19), channel_id=1, replica_groups=mesh['sp_0'=4,'sp_1'=4,'sp_2'=4,'tp'=2] {'sp_2'}, dimensions={0} | all-to-all | bytes 557056 | tf_op jit(solution)/shard_map/all_to_all | solution.py:454
  26.6 0.1 row_total.1
  26.7 5.5 %collective-permute-start.2 = (bf16[136,256]{1,0:T(8,128)(2,1)S(1)}, bf16[136,256]{1,0:T(8,128)(2,1)S(1)}, u32[]{:S(2)}, u32[]{:S(2)}) collective-permute-start(bf16[136,256]{1,0:T(8,128)(2,1)S(1)} %row_total.1), channel_id=1, source_target_pairs={{0,16},{2,18},{4,20},{6,22},{8,24},{10,26},{12,28},{14,30},{16,32}... | collective-permute-start | bytes 208904 | tf_op jit(solution)/shard_map/ppermute | solution.py:388
  32.1 2.3 %collective-permute-start.1 = (bf16[136,256]{1,0:T(8,128)(2,1)S(1)}, bf16[136,256]{1,0:T(8,128)(2,1)S(1)}, u32[]{:S(2)}, u32[]{:S(2)}) collective-permute-start(bf16[136,256]{1,0:T(8,128)(2,1)S(1)} %row_total.1), channel_id=1, source_target_pairs={{0,8},{2,10},{4,12},{6,14},{8,16},{10,18},{12,20},{14,22},{16,24},... | collective-permute-start | bytes 208904 | tf_op jit(solution)/shard_map/ppermute | solution.py:388
  34.5 1.3 collective-permute-done.1.one
  35.8 0.8 row_carry.1
  36.6 3.4 %all-to-all-start.1 = ((bf16[4,128,256]{2,1,0:T(8,128)(2,1)}), bf16[4,128,256]{2,1,0:T(8,128)(2,1)S(1)}, u32[]{:S(2)}, u32[]{:S(2)}) async-start(bf16[4,128,256]{2,1,0:T(8,128)(2,1)} %row_carry.1), calls=%async_computation.1 | async-start | bytes 524288 | tf_op jit(solution)/shard_map/all_to_all | solution.py:469
  40.0 1.0 copy-done.13
  41.1 1.0 copy-done.15
  42.1 1.0 copy-done.17
  43.2 3.5 %inner.1 = (f32[256,1024]{1,0:T(8,128)S(1)}, f32[256,1024]{1,0:T(8,128)S(1)}) custom-call(bf16[256,1024]{1,0:T(8,128)(2,1)S(1)} %copy-done.15, bf16[256,1024]{1,0:T(8,128)(2,1)S(1)} %copy-done.17, bf16[256,128]{1,0:T(8,128)(2,1)S(1)} %get-tuple-element.22.bc, bf16[256,128]{1,0:T(8,128)(2,1)S(1)} %get-tuple-element.18.cc, ...), custom_call_target="tpu_custom_call" | custom-call | flops 4000000000 | bytes 4000000 | tf_op jit(solution)/shard_map/inner/pallas_call | solution.py:457
  46.7 0.0 copy-start.19
  46.7 0.0 copy-start.22
  46.7 0.0 copy-start.5
  46.8 0.3 outer.1
  47.1 4.2 %collective-permute-start.3 = (bf16[128,1024]{1,0:T(8,128)(2,1)S(1)}, bf16[128,1024]{1,0:T(8,128)(2,1)S(1)}, u32[]{:S(2)}, u32[]{:S(2)}) collective-permute-start(bf16[128,1024]{1,0:T(8,128)(2,1)S(1)} %get-tuple-element.26), channel_id=1, source_target_pairs={{0,1},{1,0},{2,3},{3,2},{4,5},{5,4},{6,7},{7,6},{8,9},{9,8},{10,11... | collective-permute-start | bytes 786440 | tf_op jit(solution)/shard_map/ppermute | solution.py:473
  51.3 0.1 copy.29.group_w
  51.4 0.1 copy.28.chosen_w
  51.5 0.1 copy.27.chosen
  51.6 0.5 route.1
  52.1 0.3 collective-permute-done.3.got
  52.4 3.4 %copy-done = bf16[2048,2048]{1,0:T(8,128)(2,1)S(1)} copy-done((bf16[2048,2048]{1,0:T(8,128)(2,1)S(1)}, bf16[2048,2048]{1,0:T(8,128)(2,1)}, u32[]{:S(2)}) %copy-start) | copy-done | bytes 8388632
  55.8 3.7 %proj.1 = (bf16[128,2048]{1,0:T(8,128)(2,1)S(1)}, bf16[2048,512]{1,0:T(8,128)(2,1)S(1)}) custom-call(bf16[128,1024]{1,0:T(8,128)(2,1)S(1)} %get-tuple-element.25.keep, bf16[128,1024]{1,0:T(8,128)(2,1)S(1)} %collective-permute-done.3.got, bf16[2048,2048]{1,0:T(8,128)(2,1)S(1)} %copy-done, f32[2,1024]{1,0:T(2,128)S(1)} %reshape.32.gain, ...), custom_call_target="tpu_custom_call" | custom-call | tf_op jit(solution)/shard_map/proj/pallas_call | solution.py:474
  59.5 0.0 copy-start.1
  59.5 42.9 %all_to_all.21 = bf16[128,16,512]{2,1,0:T(8,128)(2,1)S(1)} all-to-all(bf16[128,16,512]{2,1,0:T(8,128)(2,1)S(1)} %bitcast.12), channel_id=1, replica_groups=mesh['sp_0'=4,'sp_1'=4,'sp_2'=4,'tp'=2] {'sp_0','sp_1','sp_2','tp'}, dimensions={0} | all-to-all | bytes 4194304 | tf_op jit(solution)/shard_map/all_to_all | solution.py:489
  102.5 5.5 %expert.1 = bf16[2048,512]{1,0:T(8,128)(2,1)S(1)} custom-call(bf16[2048,512]{1,0:T(8,128)(2,1)S(1)} %bitcast.9, bf16[1,2048,512]{2,1,0:T(8,128)(2,1)S(1)} %copy-done.1, bf16[1,2048,512]{2,1,0:T(8,128)(2,1)S(1)} %copy-done.2, bf16[1,512,2048]{2,1,0:T(8,128)(2,1)S(1)} %copy-done.3), custom_call_target="tpu_custom_call" | custom-call | tf_op jit(solution)/shard_map/expert/pallas_call | solution.py:490
  108.0 34.4 %all_to_all.22 = bf16[128,16,512]{2,1,0:T(8,128)(2,1)S(1)} all-to-all(bf16[128,16,512]{2,1,0:T(8,128)(2,1)S(1)} %bitcast.10), channel_id=1, replica_groups=mesh['sp_0'=4,'sp_1'=4,'sp_2'=4,'tp'=2] {'sp_0','sp_1','sp_2','tp'}, dimensions={0} | all-to-all | bytes 4194304 | tf_op jit(solution)/shard_map/all_to_all | solution.py:504
  142.3 2.1 %combine.1 = bf16[128,2048]{1,0:T(8,128)(2,1)} custom-call(bf16[2048,512]{1,0:T(8,128)(2,1)S(1)} %bitcast.11, bf16[128,2048]{1,0:T(8,128)(2,1)S(1)} %get-tuple-element.29.mixed, f32[128,128]{1,0:T(8,128)S(1)} %get-tuple-element.30.route), custom_call_target="tpu_custom_call" | custom-call | tf_op jit(solution)/shard_map/combine/pallas_call | solution.py:505
  (34 shorter events, 0.1 us)
Async XLA Ops:
  0.0 40.0 %copy-start.18 = (f32[16]{0:T(128)S(1)}, f32[16]{0:T(128)}, u32[]{:S(2)}) copy-start(f32[16]{0:T(128)} %param.29) | copy-start | bytes 196
  2.9 5.6 %collective-permute-start = (bf16[8,1408]{1,0:T(8,128)(2,1)S(1)}, bf16[8,1408]{1,0:T(8,128)(2,1)S(1)}, u32[]{:S(2)}, u32[]{:S(2)}) collective-permute-start(bf16[8,1408]{1,0:T(8,128)(2,1)S(1)} %pad_maximum_fusion), channel_id=1, source_target_pairs={{0,2},{2,4},{4,6},{6,8},{8,10},{10,12},{12,14},{14,16},{16,18},{18... | collective-permute-start | bytes 67592 | tf_op jit(solution)/shard_map/ppermute | solution.py:388
  8.6 1.0 copy-start.4
  9.7 0.8 copy-start.6
  10.5 0.8 copy-start.7
  11.3 0.7 copy-start.8
  12.0 0.7 copy-start.10
  12.7 0.7 copy-start.11
  13.4 0.7 copy-start.12
  16.6 0.8 copy-start.16
  17.4 18.4 %copy-start.14 = (bf16[256,1024]{1,0:T(8,128)(2,1)}, bf16[256,1024]{1,0:T(8,128)(2,1)S(1)}, u32[]{:S(2)}) copy-start(bf16[256,1024]{1,0:T(8,128)(2,1)S(1)} %get-tuple-element.20.xs) | copy-start | bytes 1572868
  26.7 7.8 %collective-permute-start.2 = (bf16[136,256]{1,0:T(8,128)(2,1)S(1)}, bf16[136,256]{1,0:T(8,128)(2,1)S(1)}, u32[]{:S(2)}, u32[]{:S(2)}) collective-permute-start(bf16[136,256]{1,0:T(8,128)(2,1)S(1)} %row_total.1), channel_id=1, source_target_pairs={{0,16},{2,18},{4,20},{6,22},{8,24},{10,26},{12,28},{14,30},{16,32}... | collective-permute-start | bytes 208904 | tf_op jit(solution)/shard_map/ppermute | solution.py:388
  32.1 3.7 %collective-permute-start.1 = (bf16[136,256]{1,0:T(8,128)(2,1)S(1)}, bf16[136,256]{1,0:T(8,128)(2,1)S(1)}, u32[]{:S(2)}, u32[]{:S(2)}) collective-permute-start(bf16[136,256]{1,0:T(8,128)(2,1)S(1)} %row_total.1), channel_id=1, source_target_pairs={{0,8},{2,10},{4,12},{6,14},{8,16},{10,18},{12,20},{14,22},{16,24},... | collective-permute-start | bytes 208904 | tf_op jit(solution)/shard_map/ppermute | solution.py:388
  36.6 10.2 %all-to-all-start.1 = ((bf16[4,128,256]{2,1,0:T(8,128)(2,1)}), bf16[4,128,256]{2,1,0:T(8,128)(2,1)S(1)}, u32[]{:S(2)}, u32[]{:S(2)}) async-start(bf16[4,128,256]{2,1,0:T(8,128)(2,1)} %row_carry.1), calls=%async_computation.1 | async-start | bytes 524288 | tf_op jit(solution)/shard_map/all_to_all | solution.py:469
  40.0 1.0 copy-start.13
  41.1 1.0 copy-start.15
  42.1 1.0 copy-start.17
  46.7 4.6 %copy-start.19 = (f32[2048]{0:T(1024)S(1)}, f32[2048]{0:T(1024)}, u32[]{:S(2)}) copy-start(f32[2048]{0:T(1024)} %param.34) | copy-start | bytes 24580
  46.7 4.6 %copy-start.20 = (f32[128,4]{0,1:T(4,128)S(1)}, f32[128,4]{0,1:T(4,128)}, u32[]{:S(2)}) copy-start(f32[128,4]{0,1:T(4,128)} %param.38) | copy-start | bytes 6148
  46.7 4.7 %copy-start.21 = (f32[128,2]{0,1:T(2,128)S(1)}, f32[128,2]{0,1:T(2,128)}, u32[]{:S(2)}) copy-start(f32[128,2]{0,1:T(2,128)} %param.39) | copy-start | bytes 3076
  46.7 4.8 %copy-start.22 = (s32[128,2]{0,1:T(2,128)S(1)}, s32[128,2]{0,1:T(2,128)}, u32[]{:S(2)}) copy-start(s32[128,2]{0,1:T(2,128)} %param.40) | copy-start | bytes 3076
  46.7 5.7 %copy-start.5 = (bf16[128,2048]{1,0:T(8,128)(2,1)S(1)}, bf16[128,2048]{1,0:T(8,128)(2,1)}, u32[]{:S(2)}) copy-start(bf16[128,2048]{1,0:T(8,128)(2,1)} %residual.1) | copy-start | bytes 1572868
  46.7 5.7 %copy-start.9 = (f32[2048]{0:T(1024)S(1)}, f32[2048]{0:T(1024)}, u32[]{:S(2)}) copy-start(f32[2048]{0:T(1024)} %param.37) | copy-start | bytes 24580
  47.1 5.4 %collective-permute-start.3 = (bf16[128,1024]{1,0:T(8,128)(2,1)S(1)}, bf16[128,1024]{1,0:T(8,128)(2,1)S(1)}, u32[]{:S(2)}, u32[]{:S(2)}) collective-permute-start(bf16[128,1024]{1,0:T(8,128)(2,1)S(1)} %get-tuple-element.26), channel_id=1, source_target_pairs={{0,1},{1,0},{2,3},{3,2},{4,5},{5,4},{6,7},{7,6},{8,9},{9,8},{10,11... | collective-permute-start | bytes 786440 | tf_op jit(solution)/shard_map/ppermute | solution.py:473
  52.4 3.4 %copy-start = (bf16[2048,2048]{1,0:T(8,128)(2,1)S(1)}, bf16[2048,2048]{1,0:T(8,128)(2,1)}, u32[]{:S(2)}) copy-start(bf16[2048,2048]{1,0:T(8,128)(2,1)} %w_hbm.1) | copy-start | bytes 25165828
  55.8 46.7 %copy-start.3 = (bf16[1,512,2048]{2,1,0:T(8,128)(2,1)S(1)}, bf16[1,512,2048]{2,1,0:T(8,128)(2,1)}, u32[]{:S(2)}) copy-start(bf16[1,512,2048]{2,1,0:T(8,128)(2,1)} %down_hbm.1) | copy-start | bytes 6291460
  59.5 43.0 %copy-start.1 = (bf16[1,2048,512]{2,1,0:T(8,128)(2,1)S(1)}, bf16[1,2048,512]{2,1,0:T(8,128)(2,1)}, u32[]{:S(2)}) copy-start(bf16[1,2048,512]{2,1,0:T(8,128)(2,1)} %gate_hbm.1) | copy-start | bytes 6291460
  59.5 43.0 %copy-start.2 = (bf16[1,2048,512]{2,1,0:T(8,128)(2,1)S(1)}, bf16[1,2048,512]{2,1,0:T(8,128)(2,1)}, u32[]{:S(2)}) copy-start(bf16[1,2048,512]{2,1,0:T(8,128)(2,1)} %up_hbm.1) | copy-start | bytes 6291460
